TPU v7x, 32 devices: a whole 2x2x4 slice. The times are simulated.
32 devices in a mesh: ep: 8 (over z, core), tp: 4 (over y, x).
Axes of the slice: x: 2, y: 2, z: 4, core: 2. Of those that a mesh axis runs over, the one named last changes fastest.
Arguments:
- tokens: bfloat16 [384, 2048], P('ep'), may hold values from -6 to 6
- retention_state: float32 [384, 16, 64, 64], P('ep', 'tp'), may hold values from -1.5 to 1.5
- lengths: int32 [384], P('ep'), may hold values from 1024 to 16383
- query_weight: bfloat16 [2048, 1024], P(None, 'tp'), may hold values from -0.125 to 0.125
- key_weight: bfloat16 [2048, 1024], P(None, 'tp'), may hold values from -0.125 to 0.125
- value_weight: bfloat16 [2048, 1024], P(None, 'tp'), may hold values from -0.125 to 0.125
- gate_weight: bfloat16 [2048, 1024], P(None, 'tp'), may hold values from -0.125 to 0.125
- out_weight: bfloat16 [1024, 2048], P(None, 'tp'), may hold values from -0.1875 to 0.1875
- first_gain: float32 [2048], replicated, may hold values from 0.1 to 1.9
- routing: int32 [384, 4], P('ep'), may hold values from 0 to 31, all different within a row; in each aligned block of 48 rows (0 to 47, 48 to 95, ...) at most 18 rows name the same one
- route_weight: float32 [384, 4], P('ep'), may hold values from 0.1 to 1
- expert_gate: bfloat16 [32, 2048, 512], P('ep', None, 'tp'), may hold values from -0.125 to 0.125
- expert_up: bfloat16 [32, 2048, 512], P('ep', None, 'tp'), may hold values from -0.125 to 0.125
- expert_down: bfloat16 [32, 512, 2048], P('ep', None, 'tp'), may hold values from -0.25 to 0.25
- shared_gate: bfloat16 [2048, 512], P(None, 'tp'), may hold values from -0.125 to 0.125
- shared_up: bfloat16 [2048, 512], P(None, 'tp'), may hold values from -0.125 to 0.125
- shared_down: bfloat16 [512, 2048], P(None, 'tp'), may hold values from -0.25 to 0.25
- side_gate: bfloat16 [2048, 256], P('ep', 'tp'), may hold values from -0.125 to 0.125
- side_up: bfloat16 [2048, 256], P('ep', 'tp'), may hold values from -0.125 to 0.125
- side_down: bfloat16 [256, 2048], P(None, 'tp'), may hold values from -0.375 to 0.375
- side_switch: bfloat16 [2048], replicated, may hold values from -0.125 to 0.125
- second_gain: float32 [2048], P('tp'), may hold values from 0.1 to 1.9
Outputs:
- output: bfloat16 [384, 2048], P('ep', 'tp')
- new_state: float32 [384, 16, 64, 64], P('ep', 'tp')
Inputs may be any that keep to these rules, and one draw needn't show every extreme that they name: `routing`: each row names 4 different experts. Among the rows of one ep index (aligned blocks of 48 rows) no expert is named by more than 18 rows, a bound that some block reaches.
All inputs are finite; a program needn't handle non-finite values.
Results may differ from a plain program's by a relative error of at most 0.013.
Values may be sent and summed in bfloat16 or wider, within the bound.
A program may use at most 64 MiB of HBM per device.

v0:
```python
import jax
import jax.numpy as jnp
from jax import lax
from jax.sharding import PartitionSpec as P

HEADS = 16
RESIDUAL_SCALE = 2.0**0.25
NORM_EPS = 1e-05
GROUP_EPS = 1e-06
ROPE_BASE = 10000.0


def rotate(vector, positions):
    half_width = vector.shape[-1] // 2
    frequency = ROPE_BASE ** (-jnp.arange(half_width, dtype=jnp.float32) / half_width)
    angles = positions.astype(jnp.float32)[:, None, None] * frequency[None, None, :]
    cosine = jnp.cos(angles)
    sine_part = jnp.sin(angles)
    first_half = vector[..., :half_width]
    second_half = vector[..., half_width:]
    return jnp.concatenate(
        [
            first_half * cosine - second_half * sine_part,
            second_half * cosine + first_half * sine_part,
        ],
        -1,
    )


def retain(
    tokens,
    retention_state,
    lengths,
    query_weight,
    key_weight,
    value_weight,
    gate_weight,
    first_head,
):
    row_count = tokens.shape[0]
    head_count = retention_state.shape[1]
    head_width = retention_state.shape[2]

    def project(weight):
        rounded = jnp.dot(tokens, weight, preferred_element_type=jnp.float32).astype(jnp.bfloat16)
        return lax.optimization_barrier(rounded).astype(jnp.float32)

    queries = rotate(project(query_weight).reshape(row_count, head_count, head_width), lengths)
    key_rows = rotate(
        project(key_weight).reshape(row_count, head_count, head_width), lengths
    ) * head_width ** (-0.5)
    values = project(value_weight).reshape(row_count, head_count, head_width)
    gate_act = project(gate_weight)
    head_index = (first_head + jnp.arange(head_count)).astype(jnp.float32)
    decays = 1.0 - 2.0 ** (-5.0 - 7.0 * head_index / (HEADS - 1))
    own_term = jnp.sum(queries * key_rows, -1, keepdims=True) * values
    carried = decays[None, :, None] * jnp.einsum(
        "bhd,bhde->bhe", queries, retention_state, precision=lax.Precision.HIGHEST
    )
    result = own_term + carried
    new_state = (
        decays[None, :, None, None] * retention_state
        + key_rows[:, :, :, None] * values[:, :, None, :]
    )
    normed = result * lax.rsqrt(jnp.mean(result * result, -1, keepdims=True) + GROUP_EPS)
    mixed_heads = (
        normed.reshape(row_count, head_count * head_width) * jax.nn.silu(gate_act)
    ).astype(jnp.bfloat16)
    return (mixed_heads, new_state)


def slot_numbers(route_ids, expert_count, capacity):
    onehot = (route_ids[..., None] == jnp.arange(expert_count, dtype=jnp.int32)).astype(jnp.int32)
    position = jnp.sum(jnp.cumsum(onehot, -2) * onehot, -1) - 1
    return route_ids * capacity + position


def on_device(
    tokens,
    retention_state,
    lengths,
    query_weight,
    key_weight,
    value_weight,
    gate_weight,
    out_weight,
    first_gain,
    routing,
    route_weight,
    expert_gate,
    expert_up,
    expert_down,
    shared_gate,
    shared_up,
    shared_down,
    side_gate,
    side_up,
    side_down,
    side_switch,
    second_gain,
):
    seq_rows = tokens.shape[0]
    model_width = tokens.shape[1]
    head_count = retention_state.shape[1]
    col_count = out_weight.shape[1]
    ep_count = lax.axis_size("ep")
    tp_rank = lax.axis_index("tp")
    col_start = tp_rank * col_count
    mixed_heads, new_state = retain(
        tokens,
        retention_state,
        lengths,
        query_weight,
        key_weight,
        value_weight,
        gate_weight,
        tp_rank * head_count,
    )
    mixing = jnp.dot(
        lax.all_gather(mixed_heads, "tp", axis=1, tiled=True),
        out_weight,
        preferred_element_type=jnp.float32,
    )
    own_cols = lax.dynamic_slice_in_dim(tokens, col_start, col_count, 1).astype(jnp.float32)
    pre_first = RESIDUAL_SCALE * own_cols + mixing
    whole_rows = lax.all_gather(pre_first, "tp", axis=1, tiled=True)
    row_mean = jnp.mean(whole_rows, -1, keepdims=True)
    square = jnp.mean(whole_rows * whole_rows, -1, keepdims=True)
    normed_full = (
        (whole_rows - row_mean) * lax.rsqrt(square - row_mean * row_mean + NORM_EPS) * first_gain
    ).astype(jnp.bfloat16)
    normed_cols = lax.dynamic_slice_in_dim(normed_full, col_start, col_count, 1)
    side_pre = jnp.dot(
        normed_full,
        lax.all_gather(side_gate, "ep", axis=0, tiled=True),
        preferred_element_type=jnp.float32,
    )
    side_lift = jnp.dot(
        normed_full,
        lax.all_gather(side_up, "ep", axis=0, tiled=True),
        preferred_element_type=jnp.float32,
    )
    side_hidden = (jax.nn.silu(side_pre) * side_lift).astype(jnp.bfloat16)
    shared_hidden = (
        jax.nn.silu(jnp.dot(normed_full, shared_gate, preferred_element_type=jnp.float32))
        * jnp.dot(normed_full, shared_up, preferred_element_type=jnp.float32)
    ).astype(jnp.bfloat16)
    shared_all, side_all = (
        lax.all_gather(shared_hidden, "tp", axis=1, tiled=True),
        lax.all_gather(side_hidden, "tp", axis=1, tiled=True),
    )
    shared_out = jnp.dot(shared_all, shared_down, preferred_element_type=jnp.float32)
    side_out = jnp.dot(side_all, side_down, preferred_element_type=jnp.float32)
    switch = jax.nn.sigmoid(jnp.dot(normed_full, side_switch, preferred_element_type=jnp.float32))
    top_count = routing.shape[1]
    local_experts = expert_gate.shape[0]
    expert_count = local_experts * ep_count
    capacity = (3 * seq_rows * top_count + expert_count - 1) // expert_count
    assigned = seq_rows * top_count
    slot_ids = slot_numbers(routing.reshape(assigned), expert_count, capacity)
    slot_hot = (
        slot_ids[:, None] == jnp.arange(expert_count * capacity, dtype=jnp.int32)[None, :]
    ).astype(jnp.bfloat16)
    token_hot = (
        (jnp.arange(assigned, dtype=jnp.int32) // top_count)[:, None]
        == jnp.arange(seq_rows, dtype=jnp.int32)[None, :]
    ).astype(jnp.bfloat16)
    every_rows, every_route = (
        lax.all_gather(normed_full, "ep", axis=0, tiled=True),
        lax.all_gather(routing, "ep", axis=0, tiled=True),
    )
    groups = every_route.reshape(ep_count, assigned)
    local_slot = (
        slot_numbers(groups, expert_count, capacity)
        - lax.axis_index("ep") * local_experts * capacity
    )
    local_hot = (
        local_slot[:, :, None]
        == jnp.arange(local_experts * capacity, dtype=jnp.int32)[None, None, :]
    ).astype(jnp.bfloat16)
    local_table = jnp.einsum(
        "gal,at->glt", local_hot, token_hot, preferred_element_type=jnp.float32
    ).astype(jnp.bfloat16)
    chosen = jnp.einsum(
        "glt,gtd->gld",
        local_table,
        every_rows.reshape(ep_count, seq_rows, model_width),
        preferred_element_type=jnp.float32,
    ).astype(jnp.bfloat16)
    slot_rows = chosen.reshape(ep_count * local_experts, capacity, model_width)
    slot_count = slot_rows.shape[1]
    grouped = slot_rows.reshape(ep_count, local_experts, slot_count, slot_rows.shape[2])
    gate_part = jnp.einsum(
        "sjcd,jdf->sjcf", grouped, expert_gate, preferred_element_type=jnp.float32
    )
    up_part = jnp.einsum("sjcd,jdf->sjcf", grouped, expert_up, preferred_element_type=jnp.float32)
    hidden = (jax.nn.silu(gate_part) * up_part).astype(jnp.bfloat16)
    hidden_all = lax.all_gather(hidden, "tp", axis=3, tiled=True)
    result = jnp.einsum(
        "sjcf,jfd->sjcd", hidden_all, expert_down, preferred_element_type=jnp.float32
    ).astype(jnp.bfloat16)
    returned = lax.all_to_all(
        result.reshape(ep_count * local_experts, slot_count, col_count),
        "ep",
        split_axis=0,
        concat_axis=0,
        tiled=True,
    )
    picked = jnp.dot(
        slot_hot,
        returned.reshape(expert_count * capacity, col_count),
        preferred_element_type=jnp.float32,
    ).reshape(seq_rows, top_count, col_count)
    routed = jnp.sum(picked * route_weight[:, :, None], 1)
    pre_second = (
        RESIDUAL_SCALE * normed_cols.astype(jnp.float32)
        + routed
        + shared_out
        + switch[:, None] * side_out
    )
    totals_second = lax.psum((jnp.sum(pre_second, -1), jnp.sum(pre_second * pre_second, -1)), "tp")
    mean_second = totals_second[0][:, None] / model_width
    square_second = totals_second[1][:, None] / model_width
    output = (
        (pre_second - mean_second)
        * lax.rsqrt(square_second - mean_second * mean_second + NORM_EPS)
        * second_gain
    ).astype(jnp.bfloat16)
    return (output, new_state)


def solution(mesh):
    return jax.shard_map(
        on_device,
        mesh=mesh,
        in_specs=(
            P("ep", None),
            P("ep", "tp", None, None),
            P("ep"),
            P(None, "tp"),
            P(None, "tp"),
            P(None, "tp"),
            P(None, "tp"),
            P(None, "tp"),
            P(),
            P("ep", None),
            P("ep", None),
            P("ep", None, "tp"),
            P("ep", None, "tp"),
            P("ep", None, "tp"),
            P(None, "tp"),
            P(None, "tp"),
            P(None, "tp"),
            P("ep", "tp"),
            P("ep", "tp"),
            P(None, "tp"),
            P(),
            P("tp"),
        ),
        out_specs=(P("ep", "tp"), P("ep", "tp", None, None)),
        check_vma=False,
    )
```

profile of v0, /device:TPU:0, one launch (start us, length us, event | category | flops | bytes accessed | tf_op | source)
XLA Modules:
  0.0 177.6 jit_solution(16361127171532134262)
XLA Ops:
  7.3 0.8 convert_element_type.78
  8.1 2.3 %convolution_convert_fusion.5 = bf16[48,256]{1,0:T(8,128)(2,1)} fusion(bf16[48,2048]{1,0:T(8,128)(2,1)} %param.22, bf16[2048,256]{1,0:T(8,128)(2,1)} %param.25), kind=kOutput, calls=%fused_computation.27 | convolution fusion | flops 50343936 | bytes 1269760 | tf_op jit(solution)/shard_map/dot_general | solution.py:45
  10.4 2.2 %convolution_convert_fusion.4 = bf16[48,256]{1,0:T(8,128)(2,1)} fusion(bf16[48,2048]{1,0:T(8,128)(2,1)} %param.22, bf16[2048,256]{1,0:T(8,128)(2,1)} %param.26), kind=kOutput, calls=%fused_computation.26 | convolution fusion | flops 50343936 | bytes 1269760 | tf_op jit(solution)/shard_map/dot_general | solution.py:45
  13.0 0.9 convolution_convert_fusion.2
  14.0 0.8 reshape.271
  14.9 0.8 reshape.269
  16.3 7.5 %fusion.59 = f32[48,4,1,64]{3,2,1,0:T(1,128)S(1)} fusion(f32[48,4,64,1]{2,3,1,0:T(1,128)S(1)} %bitcast.130, f32[48,4,64,64]{3,2,1,0:T(8,128)} %param.23), kind=kOutput, calls=%fused_computation.105 | convolution fusion | flops 9437184 | bytes 3244032 | tf_op jit(solution)/shard_map/bhd,bhde->bhe/dot_general | solution.py:57
  24.1 0.8 broadcast_multiply_fusion
  24.9 1.6 reshape.259
  26.5 0.8 fusion.47
  27.3 10.9 %all_gather.27 = bf16[48,1024]{1,0:T(8,128)(2,1)} all-gather(bf16[48,256]{1,0:T(8,128)(2,1)S(1)} %fusion.47), channel_id=1, replica_groups=mesh['ep'=8,'tp'=4] {'tp'}, dimensions={1}, use_global_device_ids=true | all-gather | bytes 122880 | tf_op jit(solution)/shard_map/all_gather | solution.py:120
  38.2 1.2 convolution_add_fusion
  39.4 9.4 %all_gather.28 = f32[48,2048]{1,0:T(8,128)S(1)} all-gather(f32[48,512]{1,0:T(8,128)S(1)} %convolution_add_fusion), channel_id=1, replica_groups=mesh['ep'=8,'tp'=4] {'tp'}, dimensions={1}, use_global_device_ids=true | all-gather | bytes 491520 | tf_op jit(solution)/shard_map/all_gather | solution.py:126
  49.0 0.8 multiply_convert_fusion
  49.9 13.2 %all-gather = s32[8,48,4]{1,2,0:T(4,128)S(1)} all-gather(s32[1,48,4]{1,2,0:T(4,128)S(1)} %bitcast.133), channel_id=1, replica_groups=mesh['ep'=8,'tp'=4] {'ep'}, dimensions={0}, use_global_device_ids=true | all-gather | bytes 6912 | tf_op jit(solution)/shard_map/all_gather | solution.py:170
  63.3 0.6 copy-done.14
  63.8 0.6 reduce-window.14
  65.0 0.6 slice.35
  65.9 4.6 %reduce-window.16 = s32[8,32,2,128]{3,1,2,0:T(8,128)S(1)} reduce-window(s32[8,32,2,128]{3,1,2,0:T(8,128)S(1)} %copy_bitcast_fusion, s32[]{:T(128)} %constant.71.clone.1), window={size=1x1x1x128 pad=0_0x0_0x0_0x127_0}, to_apply=%region_7.8 | reduce-window | flops 8323072 | bytes 524292 | tf_op jit(solution)/shard_map/reduce-window.2
  70.9 0.6 and_select_fusion
  71.5 0.8 bitcast_bitcast_fusion.1
  72.3 0.7 fusion.52
  73.0 14.4 %all_gather.33 = bf16[2048,64]{0,1:T(8,128)(2,1)S(1)} all-gather(bf16[256,64]{0,1:T(8,128)(2,1)} %param.39), channel_id=1, replica_groups=mesh['ep'=8,'tp'=4] {'ep'}, dimensions={0}, use_global_device_ids=true | all-gather | bytes 294912 | tf_op jit(solution)/shard_map/all_gather | solution.py:135
  87.4 14.6 %all_gather.34 = bf16[2048,64]{0,1:T(8,128)(2,1)S(1)} all-gather(bf16[256,64]{0,1:T(8,128)(2,1)} %param.40), channel_id=1, replica_groups=mesh['ep'=8,'tp'=4] {'ep'}, dimensions={0}, use_global_device_ids=true | all-gather | bytes 294912 | tf_op jit(solution)/shard_map/all_gather | solution.py:140
  102.2 0.6 broadcast_add_fusion
  102.7 0.8 fusion.61
  104.0 3.8 %convolution_convert_fusion = bf16[8,72,2048]{2,1,0:T(8,128)(2,1)} fusion(bf16[8,48,2048]{2,1,0:T(8,128)(2,1)} %bitcast.129, s32[8,192]{1,0:T(8,128)S(1)} %add_subtract_fusion, s32[192]{0:T(256)} %and_select_fusion), kind=kOutput, calls=%fused_computation.2 | convolution fusion | flops 125190144 | bytes 3939072 | tf_op jit(solution)/shard_map/glt,gtd->gld/dot_general | solution.py:184
  107.9 3.1 %copy.95 = bf16[8,72,2048]{2,0,1:T(8,128)(2,1)S(1)} copy(bf16[8,72,2048]{2,1,0:T(8,128)(2,1)} %convolution_convert_fusion) | data formatting | bytes 4718592 | tf_op jit(solution)/shard_map/convert_element_type | solution.py:189
  111.0 0.8 fusion.13
  111.8 0.8 copy-done.18
  112.6 0.8 fusion.23
  113.4 10.4 %all_gather.31 = bf16[8,4,18,512]{3,0,2,1:T(8,128)(2,1)S(1)} all-gather(bf16[8,4,18,128]{3,0,2,1:T(8,128)(2,1)S(1)} %fusion.23), channel_id=1, replica_groups=mesh['ep'=8,'tp'=4] {'tp'}, dimensions={3}, use_global_device_ids=true | all-gather | bytes 737280 | tf_op jit(solution)/shard_map/all_gather | solution.py:198
  123.8 0.7 fusion.10
  124.5 0.9 copy.105
  125.5 3.5 %all-to-all-start = ((bf16[32,18,512]{2,1,0:T(8,128)(2,1)}), bf16[32,18,512]{2,1,0:T(8,128)(2,1)S(1)}, u32[]{:S(2)}, u32[]{:S(2)}) async-start(bf16[32,18,512]{2,1,0:T(8,128)(2,1)} %bitcast.22), calls=%async_computation | async-start | bytes 1572864 | tf_op jit(solution)/shard_map/all_to_all | solution.py:202
  129.0 1.6 fusion.31
  130.6 0.7 reshape.288
  131.3 0.8 sub.90
  132.1 7.6 %all-gather.1 = bf16[4,64,48]{1,2,0:T(8,128)(2,1)S(1)} all-gather(bf16[1,64,48]{1,2,0:T(8,128)(2,1)} %fusion.31), channel_id=1, replica_groups=mesh['ep'=8,'tp'=4] {'tp'}, dimensions={0}, use_global_device_ids=true | all-gather | bytes 30720 | tf_op jit(solution)/shard_map/all_gather | solution.py:150
  139.8 0.7 reshape.279
  140.5 8.4 %all_gather.32 = bf16[48,512]{1,0:T(8,128)(2,1)} all-gather(bf16[48,128]{1,0:T(8,128)(2,1)S(1)} %fusion.29), channel_id=1, replica_groups=mesh['ep'=8,'tp'=4] {'tp'}, dimensions={1}, use_global_device_ids=true | all-gather | bytes 61440 | tf_op jit(solution)/shard_map/all_gather | solution.py:149
  149.0 7.4 %multiply_add_fusion = f32[48,4,64,64]{3,2,1,0:T(8,128)} fusion(f32[48,4,64,64]{3,2,1,0:T(8,128)} %param.23, f32[48,4,64]{2,1,0:T(4,128)S(1)} %reshape.273, f32[48,4,64]{2,1,0:T(4,128)S(1)} %get-tuple-element.24, f32[4]{0:T(128)} %copy-done.17), kind=kLoop, calls=%fused_computation.1 | loop fusion | flops 2359296 | bytes 6389776 | tf_op jit(solution)/shard_map/add | solution.py:62
  156.4 1.0 reshape.287
  157.4 1.4 fusion.22
  158.9 1.2 convolution_add_fusion.1
  160.1 1.0 fusion.58
  161.1 8.9 %all-reduce.2 = (f32[48]{0:T(128)S(1)}, f32[48]{0:T(128)S(1)}) all-reduce(f32[48]{0:T(128)S(1)} %get-tuple-element.5, f32[48]{0:T(128)S(1)} %get-tuple-element.4), channel_id=1, replica_groups=mesh['ep'=8,'tp'=4] {'tp'}, use_global_device_ids=true, to_apply=%region_14.15 | all-reduce | flops 96 | bytes 768 | tf_op jit(solution)/shard_map/psum | solution.py:221
  170.1 0.7 multiply_convert_fusion.1
  (78 shorter events, 3.9 us)
Async XLA Ops:
  7.2 116.6 %copy-start = (bf16[4,512,512]{2,1,0:T(8,128)(2,1)S(1)}, bf16[4,512,512]{2,1,0:T(8,128)(2,1)}, u32[]{:S(2)}) copy-start(bf16[4,512,512]{2,1,0:T(8,128)(2,1)} %param.35) | copy-start | bytes 6291460
  7.2 5.5 %copy-start.3 = (bf16[48,2048]{1,0:T(8,128)(2,1)S(1)}, bf16[48,2048]{1,0:T(8,128)(2,1)}, u32[]{:S(2)}) copy-start(bf16[48,2048]{1,0:T(8,128)(2,1)} %param.22) | copy-start | bytes 589828
  7.2 5.5 %copy-start.4 = (bf16[2048,256]{1,0:T(8,128)(2,1)S(1)}, bf16[2048,256]{1,0:T(8,128)(2,1)}, u32[]{:S(2)}) copy-start(bf16[2048,256]{1,0:T(8,128)(2,1)} %param.27) | copy-start | bytes 3145732
  7.2 96.8 %all-gather.4.cloned.1.call-start = ((), (), s32[]{:S(2)}) async-start(), calls=%async_computation.1 | async-start | bytes 1769472 | tf_op jit(solution)/shard_map/all_gather | solution.py:169
  7.3 5.7 %copy-start.5 = (bf16[2048,256]{1,0:T(8,128)(2,1)S(1)}, bf16[2048,256]{1,0:T(8,128)(2,1)}, u32[]{:S(2)}) copy-start(bf16[2048,256]{1,0:T(8,128)(2,1)} %param.28) | copy-start | bytes 3145732
  7.3 16.5 %copy-start.17 = (f32[4]{0:T(128)}, f32[4]{0:T(128)S(1)}, u32[]{:S(2)}) copy-start(f32[4]{0:T(128)S(1)} %power_subtract_fusion) | copy-start | bytes 52
  16.3 21.9 %copy-start.6 = (bf16[1024,512]{1,0:T(8,128)(2,1)S(1)}, bf16[1024,512]{1,0:T(8,128)(2,1)}, u32[]{:S(2)}) copy-start(bf16[1024,512]{1,0:T(8,128)(2,1)} %param.29) | copy-start | bytes 3145732
  23.8 25.2 %copy-start.15 = (f32[2048]{0:T(1024)S(1)}, f32[2048]{0:T(1024)}, u32[]{:S(2)}) copy-start(f32[2048]{0:T(1024)} %param.30) | copy-start | bytes 24580
  23.8 26.0 %copy-start.12 = (s32[48,4]{0,1:T(4,128)S(1)}, s32[48,4]{0,1:T(4,128)}, u32[]{:S(2)}) copy-start(s32[48,4]{0,1:T(4,128)} %param.31) | copy-start | bytes 2308
  49.8 53.0 %copy-start.1 = (bf16[48,2048]{1,0:T(8,128)(2,1)S(1)}, bf16[48,2048]{1,0:T(8,128)(2,1)}, u32[]{:S(2)}) copy-start(bf16[48,2048]{1,0:T(8,128)(2,1)} %multiply_convert_fusion) | copy-start | bytes 589828
  49.8 53.8 %copy-start.7 = (bf16[2048,128]{1,0:T(8,128)(2,1)S(1)}, bf16[2048,128]{1,0:T(8,128)(2,1)}, u32[]{:S(2)}) copy-start(bf16[2048,128]{1,0:T(8,128)(2,1)} %param.36) | copy-start | bytes 1572868
  63.3 0.6 copy-start.14
  64.4 0.6 copy-start.9
  70.9 32.9 %copy-start.8 = (bf16[2048,128]{1,0:T(8,128)(2,1)S(1)}, bf16[2048,128]{1,0:T(8,128)(2,1)}, u32[]{:S(2)}) copy-start(bf16[2048,128]{1,0:T(8,128)(2,1)} %param.37) | copy-start | bytes 1572868
  107.9 3.1 %copy-start.2 = (bf16[4,2048,128]{2,1,0:T(8,128)(2,1)S(1)}, bf16[4,2048,128]{2,1,0:T(8,128)(2,1)}, u32[]{:S(2)}) copy-start(bf16[4,2048,128]{2,1,0:T(8,128)(2,1)} %param.33) | copy-start | bytes 6291460
  111.0 1.6 copy-start.18
  124.5 24.3 %copy-start.13 = (s32[48,4]{0,1:T(4,128)S(1)}, s32[48,4]{0,1:T(4,128)}, u32[]{:S(2)}) copy-start(s32[48,4]{0,1:T(4,128)} %param.31) | copy-start | bytes 2308
  125.5 30.9 %all-to-all-start = ((bf16[32,18,512]{2,1,0:T(8,128)(2,1)}), bf16[32,18,512]{2,1,0:T(8,128)(2,1)S(1)}, u32[]{:S(2)}, u32[]{:S(2)}) async-start(bf16[32,18,512]{2,1,0:T(8,128)(2,1)} %bitcast.22), calls=%async_computation | async-start | bytes 1572864 | tf_op jit(solution)/shard_map/all_to_all | solution.py:202
  149.0 8.4 %copy-start.19 = (f32[48,4]{0,1:T(4,128)S(1)}, f32[48,4]{0,1:T(4,128)}, u32[]{:S(2)}) copy-start(f32[48,4]{0,1:T(4,128)} %param.32) | copy-start | bytes 2308
  156.4 2.5 %copy-start.11 = (bf16[48,512]{1,0:T(8,128)(2,1)S(1)}, bf16[48,512]{1,0:T(8,128)(2,1)}, u32[]{:S(2)}) copy-start(bf16[48,512]{1,0:T(8,128)(2,1)} %all_gather.32) | copy-start | bytes 147460
  156.4 3.7 %copy-start.10 = (bf16[256,512]{1,0:T(8,128)(2,1)S(1)}, bf16[256,512]{1,0:T(8,128)(2,1)}, u32[]{:S(2)}) copy-start(bf16[256,512]{1,0:T(8,128)(2,1)} %param.41) | copy-start | bytes 786436
  156.4 13.7 %copy-start.16 = (f32[512]{0:T(512)S(1)}, f32[512]{0:T(512)}, u32[]{:S(2)}) copy-start(f32[512]{0:T(512)} %param.43) | copy-start | bytes 6148
Sparse Core Ops, SparseCore 0:
  49.9 25.5 all-gather.3
where the time goes:
time: 179 us; the launch traced here: 178 us
  blocking collectives  97.9 us (55%)
  matrix products  27.1 us (15%)
  other arithmetic  20.6 us (12%)
  between operations  14.5 us (8%)
  local copies, waits for them, and re-layouts  14 us (8%)
  starting transfers between devices  3.58 us (2%)
    all_gather x1, blocking collectives, on_device(): lax.all_gather(side_up, 'ep', axis=0, tiled=True)  14.6 us
    all_gather x1, blocking collectives, on_device(): lax.all_gather(side_gate, 'ep', axis=0, tiled=True)  14.4 us
    all_gather x1, blocking collectives, on_device(): lax.all_gather(routing, 'ep', axis=0, tiled=True)  13.2 us
    all_gather x1, blocking collectives, on_device(): lax.all_gather(mixed_heads, 'tp', axis=1, tiled=True)  10.9 us
    all_gather x1, blocking collectives, on_device(): hidden_all = lax.all_gather(hidden, 'tp', axis=3, tiled=True)  10.4 us
    all_gather x1, blocking collectives, on_device(): whole_rows = lax.all_gather(pre_first, 'tp', axis=1, tiled=True)  9.44 us
    psum x1, blocking collectives, on_device(): lax.psum((jnp.sum(pre_second, -1), jnp.sum(pre_second * pre_second, -1)),...  8.93 us
    all_gather x1, blocking collectives, on_device(): lax.all_gather(shared_hidden, 'tp', axis=1, tiled=True)  8.35 us
  transfers between devices with their start and end apart: 2, of which 0 were waited for; matrix products, arithmetic and copies ran while one was open for 13% of the time, Pallas kernels for 0%

commit v1 on v0

--- a/solution.py
+++ b/solution.py
@@ -2,6 +2,7 @@
 import jax.numpy as jnp
 from jax import lax
 from jax.sharding import PartitionSpec as P
+from jax.lax import all_gather
 
 HEADS = 16
 RESIDUAL_SCALE = 2.0**0.25
@@ -116,11 +117,8 @@
         gate_weight,
         tp_rank * head_count,
     )
-    mixing = jnp.dot(
-        lax.all_gather(mixed_heads, "tp", axis=1, tiled=True),
-        out_weight,
-        preferred_element_type=jnp.float32,
-    )
+    _draft_wires = lambda row_data: jnp.concatenate(all_gather(row_data, "tp"), axis=1)
+    mixing = jnp.dot(_draft_wires(mixed_heads), out_weight, preferred_element_type=jnp.float32)
     own_cols = lax.dynamic_slice_in_dim(tokens, col_start, col_count, 1).astype(jnp.float32)
     pre_first = RESIDUAL_SCALE * own_cols + mixing
     whole_rows = lax.all_gather(pre_first, "tp", axis=1, tiled=True)

time: 179 us -> 178 us (level)
    unnamed x43 -> x44, local copies, waits for them, and re-layouts: 3.35 us -> 4.01 us
where the time goes in v1:
time: 178 us; the launch traced here: 177 us
  blocking collectives  96.8 us (54%)
  matrix products  27.1 us (15%)
  other arithmetic  20.6 us (12%)
  local copies, waits for them, and re-layouts  14.7 us (8%)
  between operations  14.5 us (8%)
  starting transfers between devices  3.58 us (2%)
    all_gather x1, blocking collectives, on_device(): lax.all_gather(side_up, 'ep', axis=0, tiled=True)  14.6 us
    all_gather x1, blocking collectives, on_device(): lax.all_gather(side_gate, 'ep', axis=0, tiled=True)  14.4 us
    all_gather x1, blocking collectives, on_device(): lax.all_gather(routing, 'ep', axis=0, tiled=True)  13.2 us
    all_gather x1, blocking collectives, on_device(): hidden_all = lax.all_gather(hidden, 'tp', axis=3, tiled=True)  10.4 us
    all_gather x1, blocking collectives, on_device(): all_gather(row_data, 'tp')  9.84 us
    all_gather x1, blocking collectives, on_device(): whole_rows = lax.all_gather(pre_first, 'tp', axis=1, tiled=True)  9.49 us
    psum x1, blocking collectives, on_device(): lax.psum((jnp.sum(pre_second, -1), jnp.sum(pre_second * pre_second, -1)),...  8.93 us
    all_gather x1, blocking collectives, on_device(): lax.all_gather(shared_hidden, 'tp', axis=1, tiled=True)  8.3 us
  transfers between devices with their start and end apart: 2, of which 0 were waited for; matrix products, arithmetic and copies ran while one was open for 13% of the time, Pallas kernels for 0%

profile of v1, /device:TPU:0, one launch (start us, length us, event | category | flops | bytes accessed | tf_op | source)
XLA Modules:
  0.0 177.3 jit_solution(6277647999311556806)
XLA Ops:
  7.3 0.8 convert_element_type.78
  8.1 2.3 %convolution_convert_fusion.5 = bf16[48,256]{1,0:T(8,128)(2,1)} fusion(bf16[48,2048]{1,0:T(8,128)(2,1)} %param.22, bf16[2048,256]{1,0:T(8,128)(2,1)} %param.25), kind=kOutput, calls=%fused_computation.27 | convolution fusion | flops 50343936 | bytes 1269760 | tf_op jit(solution)/shard_map/dot_general | solution.py:46
  10.4 2.2 %convolution_convert_fusion.4 = bf16[48,256]{1,0:T(8,128)(2,1)} fusion(bf16[48,2048]{1,0:T(8,128)(2,1)} %param.22, bf16[2048,256]{1,0:T(8,128)(2,1)} %param.26), kind=kOutput, calls=%fused_computation.26 | convolution fusion | flops 50343936 | bytes 1269760 | tf_op jit(solution)/shard_map/dot_general | solution.py:46
  13.0 0.9 convolution_convert_fusion.2
  14.0 0.8 reshape.279
  14.9 0.8 reshape.277
  16.3 7.5 %fusion.59 = f32[48,4,1,64]{3,2,1,0:T(1,128)S(1)} fusion(f32[48,4,64,1]{2,3,1,0:T(1,128)S(1)} %bitcast.134, f32[48,4,64,64]{3,2,1,0:T(8,128)} %param.23), kind=kOutput, calls=%fused_computation.105 | convolution fusion | flops 9437184 | bytes 3244032 | tf_op jit(solution)/shard_map/bhd,bhde->bhe/dot_general | solution.py:58
  24.1 0.8 broadcast_multiply_fusion
  24.9 1.6 reshape.265
  26.5 0.8 fusion.47
  27.3 9.8 %all-gather = bf16[192,256]{1,0:T(8,128)(2,1)S(1)} all-gather(bf16[48,256]{1,0:T(8,128)(2,1)S(1)} %fusion.47), channel_id=2, replica_groups=mesh['ep'=8,'tp'=4] {'tp'}, dimensions={0}, use_global_device_ids=true | all-gather | bytes 122880 | tf_op jit(solution)/shard_map/all_gather | solution.py:120
  37.2 0.7 copy.115
  37.9 1.2 convolution_add_fusion
  39.1 9.5 %all_gather.32 = f32[48,2048]{1,0:T(8,128)S(1)} all-gather(f32[48,512]{1,0:T(8,128)S(1)} %convolution_add_fusion), channel_id=1, replica_groups=mesh['ep'=8,'tp'=4] {'tp'}, dimensions={1}, use_global_device_ids=true | all-gather | bytes 491520 | tf_op jit(solution)/shard_map/all_gather | solution.py:124
  48.7 0.8 multiply_convert_fusion
  49.6 13.2 %all-gather.1 = s32[8,48,4]{1,2,0:T(4,128)S(1)} all-gather(s32[1,48,4]{1,2,0:T(4,128)S(1)} %bitcast.140), channel_id=1, replica_groups=mesh['ep'=8,'tp'=4] {'ep'}, dimensions={0}, use_global_device_ids=true | all-gather | bytes 6912 | tf_op jit(solution)/shard_map/all_gather | solution.py:168
  63.6 0.6 reduce-window.14
  64.8 0.6 slice.35
  65.6 4.6 %reduce-window.16 = s32[8,32,2,128]{3,1,2,0:T(8,128)S(1)} reduce-window(s32[8,32,2,128]{3,1,2,0:T(8,128)S(1)} %copy_bitcast_fusion, s32[]{:T(128)} %constant.71.clone.1), window={size=1x1x1x128 pad=0_0x0_0x0_0x127_0}, to_apply=%region_7.8 | reduce-window | flops 8323072 | bytes 524292 | tf_op jit(solution)/shard_map/reduce-window.2
  70.6 0.6 and_select_fusion
  71.2 0.8 bitcast_bitcast_fusion.1
  72.0 0.7 fusion.52
  72.7 14.4 %all_gather.37 = bf16[2048,64]{0,1:T(8,128)(2,1)S(1)} all-gather(bf16[256,64]{0,1:T(8,128)(2,1)} %param.39), channel_id=1, replica_groups=mesh['ep'=8,'tp'=4] {'ep'}, dimensions={0}, use_global_device_ids=true | all-gather | bytes 294912 | tf_op jit(solution)/shard_map/all_gather | solution.py:133
  87.1 14.6 %all_gather.38 = bf16[2048,64]{0,1:T(8,128)(2,1)S(1)} all-gather(bf16[256,64]{0,1:T(8,128)(2,1)} %param.40), channel_id=1, replica_groups=mesh['ep'=8,'tp'=4] {'ep'}, dimensions={0}, use_global_device_ids=true | all-gather | bytes 294912 | tf_op jit(solution)/shard_map/all_gather | solution.py:138
  101.9 0.6 broadcast_add_fusion
  102.5 0.8 fusion.61
  103.8 3.8 %convolution_convert_fusion = bf16[8,72,2048]{2,1,0:T(8,128)(2,1)} fusion(bf16[8,48,2048]{2,1,0:T(8,128)(2,1)} %bitcast.133, s32[8,192]{1,0:T(8,128)S(1)} %add_subtract_fusion, s32[192]{0:T(256)} %and_select_fusion), kind=kOutput, calls=%fused_computation.2 | convolution fusion | flops 125190144 | bytes 3939072 | tf_op jit(solution)/shard_map/glt,gtd->gld/dot_general | solution.py:182
  107.6 3.1 %copy.99 = bf16[8,72,2048]{2,0,1:T(8,128)(2,1)S(1)} copy(bf16[8,72,2048]{2,1,0:T(8,128)(2,1)} %convolution_convert_fusion) | data formatting | bytes 4718592 | tf_op jit(solution)/shard_map/convert_element_type | solution.py:187
  110.7 0.8 fusion.13
  111.5 0.8 copy-done.18
  112.3 0.8 fusion.23
  113.1 10.4 %all_gather.35 = bf16[8,4,18,512]{3,0,2,1:T(8,128)(2,1)S(1)} all-gather(bf16[8,4,18,128]{3,0,2,1:T(8,128)(2,1)S(1)} %fusion.23), channel_id=1, replica_groups=mesh['ep'=8,'tp'=4] {'tp'}, dimensions={3}, use_global_device_ids=true | all-gather | bytes 737280 | tf_op jit(solution)/shard_map/all_gather | solution.py:196
  123.5 0.7 fusion.10
  124.2 0.9 copy.109
  125.1 3.5 %all-to-all-start = ((bf16[32,18,512]{2,1,0:T(8,128)(2,1)}), bf16[32,18,512]{2,1,0:T(8,128)(2,1)S(1)}, u32[]{:S(2)}, u32[]{:S(2)}) async-start(bf16[32,18,512]{2,1,0:T(8,128)(2,1)} %bitcast.24), calls=%async_computation | async-start | bytes 1572864 | tf_op jit(solution)/shard_map/all_to_all | solution.py:200
  128.7 1.6 fusion.31
  130.2 0.7 reshape.297
  130.9 0.8 sub.90
  131.8 7.7 %all-gather.2 = bf16[4,64,48]{1,2,0:T(8,128)(2,1)S(1)} all-gather(bf16[1,64,48]{1,2,0:T(8,128)(2,1)} %fusion.31), channel_id=1, replica_groups=mesh['ep'=8,'tp'=4] {'tp'}, dimensions={0}, use_global_device_ids=true | all-gather | bytes 30720 | tf_op jit(solution)/shard_map/all_gather | solution.py:148
  139.5 0.7 reshape.288
  140.2 8.3 %all_gather.36 = bf16[48,512]{1,0:T(8,128)(2,1)} all-gather(bf16[48,128]{1,0:T(8,128)(2,1)S(1)} %fusion.29), channel_id=1, replica_groups=mesh['ep'=8,'tp'=4] {'tp'}, dimensions={1}, use_global_device_ids=true | all-gather | bytes 61440 | tf_op jit(solution)/shard_map/all_gather | solution.py:147
  148.7 7.4 %multiply_add_fusion = f32[48,4,64,64]{3,2,1,0:T(8,128)} fusion(f32[48,4,64,64]{3,2,1,0:T(8,128)} %param.23, f32[48,4,64]{2,1,0:T(4,128)S(1)} %reshape.281, f32[48,4,64]{2,1,0:T(4,128)S(1)} %get-tuple-element.24, f32[4]{0:T(128)} %copy-done.17), kind=kLoop, calls=%fused_computation.1 | loop fusion | flops 2359296 | bytes 6389776 | tf_op jit(solution)/shard_map/add | solution.py:63
  156.1 1.0 reshape.296
  157.1 1.4 fusion.22
  158.5 1.2 convolution_add_fusion.1
  159.8 1.0 fusion.58
  160.8 8.9 %all-reduce.2 = (f32[48]{0:T(128)S(1)}, f32[48]{0:T(128)S(1)}) all-reduce(f32[48]{0:T(128)S(1)} %get-tuple-element.5, f32[48]{0:T(128)S(1)} %get-tuple-element.4), channel_id=1, replica_groups=mesh['ep'=8,'tp'=4] {'tp'}, use_global_device_ids=true, to_apply=%region_14.15 | all-reduce | flops 96 | bytes 768 | tf_op jit(solution)/shard_map/psum | solution.py:219
  169.8 0.7 multiply_convert_fusion.1
  (80 shorter events, 4.5 us)
Async XLA Ops:
  7.2 116.3 %copy-start = (bf16[4,512,512]{2,1,0:T(8,128)(2,1)S(1)}, bf16[4,512,512]{2,1,0:T(8,128)(2,1)}, u32[]{:S(2)}) copy-start(bf16[4,512,512]{2,1,0:T(8,128)(2,1)} %param.35) | copy-start | bytes 6291460
  7.2 5.5 %copy-start.3 = (bf16[48,2048]{1,0:T(8,128)(2,1)S(1)}, bf16[48,2048]{1,0:T(8,128)(2,1)}, u32[]{:S(2)}) copy-start(bf16[48,2048]{1,0:T(8,128)(2,1)} %param.22) | copy-start | bytes 589828
  7.2 5.5 %copy-start.4 = (bf16[2048,256]{1,0:T(8,128)(2,1)S(1)}, bf16[2048,256]{1,0:T(8,128)(2,1)}, u32[]{:S(2)}) copy-start(bf16[2048,256]{1,0:T(8,128)(2,1)} %param.27) | copy-start | bytes 3145732
  7.2 96.6 %all-gather.5.cloned.1.call-start = ((), (), s32[]{:S(2)}) async-start(), calls=%async_computation.1 | async-start | bytes 1769472 | tf_op jit(solution)/shard_map/all_gather | solution.py:167
  7.3 5.7 %copy-start.5 = (bf16[2048,256]{1,0:T(8,128)(2,1)S(1)}, bf16[2048,256]{1,0:T(8,128)(2,1)}, u32[]{:S(2)}) copy-start(bf16[2048,256]{1,0:T(8,128)(2,1)} %param.28) | copy-start | bytes 3145732
  7.3 16.5 %copy-start.17 = (f32[4]{0:T(128)}, f32[4]{0:T(128)S(1)}, u32[]{:S(2)}) copy-start(f32[4]{0:T(128)S(1)} %power_subtract_fusion) | copy-start | bytes 52
  16.3 21.5 %copy-start.6 = (bf16[1024,512]{1,0:T(8,128)(2,1)S(1)}, bf16[1024,512]{1,0:T(8,128)(2,1)}, u32[]{:S(2)}) copy-start(bf16[1024,512]{1,0:T(8,128)(2,1)} %param.29) | copy-start | bytes 3145732
  23.8 24.9 %copy-start.15 = (f32[2048]{0:T(1024)S(1)}, f32[2048]{0:T(1024)}, u32[]{:S(2)}) copy-start(f32[2048]{0:T(1024)} %param.30) | copy-start | bytes 24580
  23.8 25.7 %copy-start.12 = (s32[48,4]{0,1:T(4,128)S(1)}, s32[48,4]{0,1:T(4,128)}, u32[]{:S(2)}) copy-start(s32[48,4]{0,1:T(4,128)} %param.31) | copy-start | bytes 2308
  49.5 53.0 %copy-start.1 = (bf16[48,2048]{1,0:T(8,128)(2,1)S(1)}, bf16[48,2048]{1,0:T(8,128)(2,1)}, u32[]{:S(2)}) copy-start(bf16[48,2048]{1,0:T(8,128)(2,1)} %multiply_convert_fusion) | copy-start | bytes 589828
  49.5 53.8 %copy-start.7 = (bf16[2048,128]{1,0:T(8,128)(2,1)S(1)}, bf16[2048,128]{1,0:T(8,128)(2,1)}, u32[]{:S(2)}) copy-start(bf16[2048,128]{1,0:T(8,128)(2,1)} %param.36) | copy-start | bytes 1572868
  63.0 0.6 copy-start.14
  64.1 0.6 copy-start.9
  70.6 32.9 %copy-start.8 = (bf16[2048,128]{1,0:T(8,128)(2,1)S(1)}, bf16[2048,128]{1,0:T(8,128)(2,1)}, u32[]{:S(2)}) copy-start(bf16[2048,128]{1,0:T(8,128)(2,1)} %param.37) | copy-start | bytes 1572868
  107.6 3.1 %copy-start.2 = (bf16[4,2048,128]{2,1,0:T(8,128)(2,1)S(1)}, bf16[4,2048,128]{2,1,0:T(8,128)(2,1)}, u32[]{:S(2)}) copy-start(bf16[4,2048,128]{2,1,0:T(8,128)(2,1)} %param.33) | copy-start | bytes 6291460
  110.7 1.6 copy-start.18
  124.2 24.3 %copy-start.13 = (s32[48,4]{0,1:T(4,128)S(1)}, s32[48,4]{0,1:T(4,128)}, u32[]{:S(2)}) copy-start(s32[48,4]{0,1:T(4,128)} %param.31) | copy-start | bytes 2308
  125.1 30.9 %all-to-all-start = ((bf16[32,18,512]{2,1,0:T(8,128)(2,1)}), bf16[32,18,512]{2,1,0:T(8,128)(2,1)S(1)}, u32[]{:S(2)}, u32[]{:S(2)}) async-start(bf16[32,18,512]{2,1,0:T(8,128)(2,1)} %bitcast.24), calls=%async_computation | async-start | bytes 1572864 | tf_op jit(solution)/shard_map/all_to_all | solution.py:200
  148.7 8.4 %copy-start.19 = (f32[48,4]{0,1:T(4,128)S(1)}, f32[48,4]{0,1:T(4,128)}, u32[]{:S(2)}) copy-start(f32[48,4]{0,1:T(4,128)} %param.32) | copy-start | bytes 2308
  156.1 2.5 %copy-start.11 = (bf16[48,512]{1,0:T(8,128)(2,1)S(1)}, bf16[48,512]{1,0:T(8,128)(2,1)}, u32[]{:S(2)}) copy-start(bf16[48,512]{1,0:T(8,128)(2,1)} %all_gather.36) | copy-start | bytes 147460
  156.1 3.7 %copy-start.10 = (bf16[256,512]{1,0:T(8,128)(2,1)S(1)}, bf16[256,512]{1,0:T(8,128)(2,1)}, u32[]{:S(2)}) copy-start(bf16[256,512]{1,0:T(8,128)(2,1)} %param.41) | copy-start | bytes 786436
  156.1 13.7 %copy-start.16 = (f32[512]{0:T(512)S(1)}, f32[512]{0:T(512)}, u32[]{:S(2)}) copy-start(f32[512]{0:T(512)} %param.43) | copy-start | bytes 6148
Sparse Core Ops, SparseCore 0:
  49.7 25.5 all-gather.4
